TPU v7x, 32 devices: a whole 2x2x4 slice. The times are simulated.
32 devices in a mesh: grp: 2 (over y), ep: 8 (over z, x), tp: 2 (over core).
Axes of the slice: x: 2, y: 2, z: 4, core: 2. Of those that a mesh axis runs over, the one named last changes fastest.
Arguments:
- hidden_state: bfloat16 [1024, 1024], P(('grp', 'ep'), 'tp'), parts along dimension 0, may hold values from -6 to 6
- expert_ids: int32 [1024, 4], P(('grp', 'ep')), parts along dimension 0, may hold values from 0 to 7, all different within a row; in each aligned block of 64 rows (0 to 63, 64 to 127, ...) at most 64 rows name the same one
- route_weight: float32 [1024, 4], P(('grp', 'ep')), parts along dimension 0, may hold values from 0.1 to 1
- gate_matrix: bfloat16 [8, 1024, 2048], P('ep', None, 'tp'), may hold values from -0.1875 to 0.1875
- up_matrix: bfloat16 [8, 1024, 2048], P('ep', None, 'tp'), may hold values from -0.1875 to 0.1875
- down_matrix: bfloat16 [8, 2048, 1024], P('ep', 'tp'), may hold values from -2 to 2
- norm_gain: float32 [1024], P('tp'), may hold values from 0.1 to 1.9
Outputs:
- normed_out: bfloat16 [1024, 1024], P(('grp', 'ep'), 'tp'), parts along dimension 0
There are 2 independent parts, one for each index of `grp`. A program takes and returns all parts, laid end to end along the dimension named above; an argument that names none is the same for every part. Nothing has to cross between parts.
Inputs may be any that keep to these rules, and one draw needn't show every extreme that they name: `expert_ids`: each row names 4 different experts. Within the rows of one index of ep (aligned blocks of 64 rows) no expert is named by more than 64 rows, and in some blocks one expert is named by exactly 64 rows. Every expert is named by some row.
All inputs are finite; a program needn't handle non-finite values.
Results may differ from a plain program's by a relative error of at most 0.0065.
Values may be sent and summed in bfloat16 or wider, within the bound.
A program may use at most 64 MiB of HBM per device.

v0:
```python
import jax
import jax.numpy as jnp
from jax import lax
from jax.sharding import PartitionSpec as P

D = 1024
norm_eps = 1e-05


def slot_numbers(block_ids, expert_count):
    onehot = (block_ids[..., None] == jnp.arange(expert_count, dtype=jnp.int32)).astype(jnp.int32)
    earlier = jnp.cumsum(onehot, axis=-2) - onehot
    return jnp.sum(earlier * onehot, axis=-1)


def expert_rows(buffer, gate_matrix, up_matrix, down_matrix):
    sources, item_count, feature_count = buffer.shape
    token_rows = buffer.reshape(sources * item_count, feature_count)
    gate_pre = jnp.dot(token_rows, gate_matrix[0], preferred_element_type=jnp.float32)
    up_pre = jnp.dot(token_rows, up_matrix[0], preferred_element_type=jnp.float32)
    activated = (jax.nn.silu(gate_pre) * up_pre).astype(jnp.bfloat16)
    partial_value = jnp.dot(activated, down_matrix[0], preferred_element_type=jnp.float32)
    summed = lax.psum_scatter(
        partial_value.reshape(sources, item_count, feature_count).astype(jnp.bfloat16),
        "tp",
        scatter_dimension=2,
        tiled=True,
    )
    return summed


def shards(hidden_state, expert_ids, route_weight, gate_matrix, up_matrix, down_matrix, norm_gain):
    tok_count, top_count = expert_ids.shape
    expert_count = lax.axis_size("ep")
    capacity = max(2, 2 * tok_count * top_count // expert_count)
    slot_total = expert_count * capacity
    slot_rank = slot_numbers(expert_ids.reshape(1, tok_count * top_count), expert_count)
    slot_index = expert_ids * capacity + slot_rank.reshape(tok_count, top_count)
    positions = jnp.arange(slot_total, dtype=jnp.int32)
    matches = slot_index[:, :, None] == positions[None, None, :]
    placing = jnp.transpose(jnp.any(matches, axis=1)).astype(jnp.bfloat16)
    combine = jnp.sum(jnp.where(matches, route_weight[:, :, None], 0.0), axis=1)
    outgoing = jnp.dot(placing, hidden_state, preferred_element_type=jnp.float32).astype(
        jnp.bfloat16
    )
    answers = expert_rows(
        lax.all_gather(
            lax.all_to_all(
                outgoing.reshape(expert_count, capacity, hidden_state.shape[1]),
                "ep",
                split_axis=0,
                concat_axis=0,
                tiled=True,
            ),
            "tp",
            axis=2,
            tiled=True,
        ),
        gate_matrix,
        up_matrix,
        down_matrix,
    )
    returned = lax.all_to_all(answers, "ep", split_axis=0, concat_axis=0, tiled=True)
    combined = jnp.dot(
        combine,
        returned.reshape(slot_total, returned.shape[2]).astype(jnp.float32),
        precision=lax.Precision.HIGHEST,
    )
    local_squares = jnp.sum(combined * combined, axis=1)
    total_squares = lax.psum(local_squares, "tp")
    inverse_rms = lax.rsqrt(total_squares / D + norm_eps)
    return (combined * inverse_rms[:, None] * norm_gain).astype(jnp.bfloat16)


def solution(mesh):
    placed = (
        P(("grp", "ep"), "tp"),
        P(("grp", "ep"), None),
        P(("grp", "ep"), None),
        P("ep", None, "tp"),
        P("ep", None, "tp"),
        P("ep", "tp", None),
        P("tp"),
    )
    return jax.shard_map(
        shards, mesh=mesh, in_specs=placed, out_specs=P(("grp", "ep"), "tp"), check_vma=False
    )
```

profile of v0, /device:TPU:0, one launch (start us, length us, event | category | flops | bytes accessed | tf_op | source)
XLA Modules:
  0.0 88.2 jit_solution(9417557024511087397)
XLA Ops:
  6.5 0.9 %copy.18 = s32[64,4]{1,0:T(8,128)S(1)} copy(s32[64,4]{0,1:T(4,128)} %param.8) | data formatting | bytes 2048 | tf_op args[1]
  7.5 0.1 eq.40
  7.6 0.6 reduce-window.6
  8.2 0.2 slice_reduce_fusion
  8.4 0.1 fusion.13
  8.5 0.1 reshape.139
  8.6 0.1 copy.19
  8.7 0.7 multiply_add_fusion
  9.4 0.1 fusion.11
  9.5 1.2 %convolution_convert_fusion = bf16[512,512]{1,0:T(8,128)(2,1)S(1)} fusion(pred[64,512]{1,0:T(8,128)(4,1)S(1)} %fusion.11, bf16[64,512]{1,0:T(8,128)(2,1)} %param.7), kind=kOutput, calls=%fused_computation.8 | convolution fusion | flops 33816576 | bytes 622592 | tf_op jit(solution)/shard_map/dot_general | solution.py:43
  10.7 21.7 %all_to_all.10 = bf16[8,64,512]{2,1,0:T(8,128)(2,1)} all-to-all(bf16[8,64,512]{2,1,0:T(8,128)(2,1)S(1)} %bitcast.41), channel_id=1, replica_groups=mesh['grp'=2,'ep'=8,'tp'=2] {'ep'}, dimensions={0} | all-to-all | bytes 1048576 | tf_op jit(solution)/shard_map/all_to_all | solution.py:48
  32.5 0.0 reduce-scatter.2.cloned.1.call-start
  32.5 8.2 %all-gather.2.cloned.1.call-done = bf16[8,64,1024]{2,1,0:T(8,128)(2,1)} async-done(((bf16[8,64,512]{2,1,0:T(8,128)(2,1)}), bf16[8,64,1024]{2,1,0:T(8,128)(2,1)}) %all-gather.2.cloned.1.call-update) | async-done | bytes 1048592 | tf_op jit(solution)/shard_map/all_gather | solution.py:47
  40.7 2.6 %fusion.4 = f32[512,1024]{1,0:T(8,128)S(1)} fusion(bf16[512,1024]{1,0:T(8,128)(2,1)} %bitcast.43, bf16[1,1024,1024]{2,1,0:T(8,128)(2,1)S(1)} %copy-done), kind=kOutput, calls=%fused_computation.4 | convolution fusion | flops 1073741824 | bytes 5242880 | tf_op jit(solution)/shard_map/dot_general | solution.py:19
  43.4 1.4 %multiply_convert_fusion = bf16[512,1024]{1,0:T(8,128)(2,1)S(1)} fusion(f32[512,1024]{1,0:T(8,128)S(1)} %fusion.4, bf16[512,1024]{1,0:T(8,128)(2,1)S(1)} %bitcast.44, bf16[1,1024,1024]{2,1,0:T(8,128)(2,1)S(1)} %copy-done.3), kind=kOutput, calls=%fused_computation.6 | convolution fusion | flops 1076887552 | bytes 6291456 | tf_op jit(solution)/shard_map/dot_general | solution.py:20
  44.7 0.2 copy-done.4
  44.9 2.2 %fusion.8 = bf16[8,64,1024]{2,1,0:T(8,128)(2,1)} fusion(bf16[8,64,1024]{2,1,0:T(8,128)(2,1)S(1)} %bitcast.45, bf16[1,1024,1024]{2,1,0:T(8,128)(2,1)S(1)} %copy-done.4), kind=kOutput, calls=%fused_computation.7 | convolution fusion | flops 1074266112 | bytes 4194304 | tf_op jit(solution)/shard_map/dot_general | solution.py:22
  47.2 9.7 %reduce-scatter.2.cloned.1.call-done = bf16[8,64,512]{2,1,0:T(8,128)(2,1)} async-done(((bf16[8,64,1024]{2,1,0:T(8,128)(2,1)}), bf16[8,64,512]{2,1,0:T(8,128)(2,1)}) %reduce-scatter.2.cloned.1.call-update) | async-done | bytes 524304 | tf_op jit(solution)/shard_map/reduce_scatter | solution.py:23
  56.9 5.8 %all-to-all-start.1 = ((bf16[8,64,512]{2,1,0:T(8,128)(2,1)}), bf16[8,64,512]{2,1,0:T(8,128)(2,1)S(1)}, u32[]{:S(2)}, u32[]{:S(2)}) async-start(bf16[8,64,512]{2,1,0:T(8,128)(2,1)} %reduce-scatter.2.cloned.1.call-done), calls=%async_computation.2 | async-start | bytes 1048576 | tf_op jit(solution)/shard_map/all_to_all | solution.py:63
  62.7 0.1 select_reduce_fusion
  62.8 14.8 %all-to-all-done.1 = bf16[8,64,512]{2,1,0:T(8,128)(2,1)S(1)} async-done(((bf16[8,64,512]{2,1,0:T(8,128)(2,1)}), bf16[8,64,512]{2,1,0:T(8,128)(2,1)S(1)}, u32[]{:S(2)}, u32[]{:S(2)}) %all-to-all-start.1) | async-done | bytes 524320 | tf_op jit(solution)/shard_map/all_to_all | solution.py:63
  77.6 0.5 multiply_reduce_fusion
  78.1 2.5 %psum.7 = f32[64]{0:T(128)S(1)} all-reduce(f32[64]{0:T(128)S(1)} %get-tuple-element.5), channel_id=1, replica_groups=mesh['grp'=2,'ep'=8,'tp'=2] {'tp'}, use_global_device_ids=true, to_apply=%region_7.8 | all-reduce | flops 64 | bytes 512 | tf_op jit(solution)/shard_map/psum | solution.py:70
  80.6 0.7 multiply_convert_fusion.1
  (18 shorter events, 0.1 us)
Async XLA Ops:
  6.5 34.2 %copy-start = (bf16[1,1024,1024]{2,1,0:T(8,128)(2,1)S(1)}, bf16[1,1024,1024]{2,1,0:T(8,128)(2,1)}, u32[]{:S(2)}) copy-start(bf16[1,1024,1024]{2,1,0:T(8,128)(2,1)} %param.10) | copy-start | bytes 6291460
  6.5 34.2 %all-gather.2.cloned.1.call-start = ((), (), s32[]{:S(2)}) async-start(), calls=%async_computation.3 | async-start | bytes 1572864 | tf_op jit(solution)/shard_map/all_gather | solution.py:47
  32.5 24.4 %reduce-scatter.2.cloned.1.call-start = ((), (), s32[]{:S(2)}) async-start(), calls=%async_computation.4 | async-start | bytes 1572864 | tf_op jit(solution)/shard_map/reduce_scatter | solution.py:23
  40.7 2.6 %copy-start.3 = (bf16[1,1024,1024]{2,1,0:T(8,128)(2,1)S(1)}, bf16[1,1024,1024]{2,1,0:T(8,128)(2,1)}, u32[]{:S(2)}) copy-start(bf16[1,1024,1024]{2,1,0:T(8,128)(2,1)} %param.11) | copy-start | bytes 6291460
  40.7 2.6 %copy-start.5 = (bf16[8,64,1024]{2,1,0:T(8,128)(2,1)S(1)}, bf16[8,64,1024]{2,1,0:T(8,128)(2,1)}, u32[]{:S(2)}) copy-start(bf16[8,64,1024]{2,1,0:T(8,128)(2,1)} %all-gather.2.cloned.1.call-done) | copy-start | bytes 3145732
  43.3 1.6 %copy-start.4 = (bf16[1,1024,1024]{2,1,0:T(8,128)(2,1)S(1)}, bf16[1,1024,1024]{2,1,0:T(8,128)(2,1)}, u32[]{:S(2)}) copy-start(bf16[1,1024,1024]{2,1,0:T(8,128)(2,1)} %param.12) | copy-start | bytes 6291460
  47.2 15.5 %copy-start.1 = (f32[64,4]{0,1:T(4,128)S(1)}, f32[64,4]{0,1:T(4,128)}, u32[]{:S(2)}) copy-start(f32[64,4]{0,1:T(4,128)} %param.9) | copy-start | bytes 3076
  47.2 33.4 %copy-start.2 = (f32[512]{0:T(512)S(1)}, f32[512]{0:T(512)}, u32[]{:S(2)}) copy-start(f32[512]{0:T(512)} %param.13) | copy-start | bytes 6148
  56.9 20.7 %all-to-all-start.1 = ((bf16[8,64,512]{2,1,0:T(8,128)(2,1)}), bf16[8,64,512]{2,1,0:T(8,128)(2,1)S(1)}, u32[]{:S(2)}, u32[]{:S(2)}) async-start(bf16[8,64,512]{2,1,0:T(8,128)(2,1)} %reduce-scatter.2.cloned.1.call-done), calls=%async_computation.2 | async-start | bytes 1048576 | tf_op jit(solution)/shard_map/all_to_all | solution.py:63
Sparse Core Ops, SparseCore 0:
  32.6 8.0 all-gather.1
  47.3 9.5 reduce-scatter.1
where the time goes:
time: 88.5 us; the launch traced here: 88.2 us
  waiting for transfers between devices  32.7 us (37%)
  blocking collectives  24.2 us (27%)
  between operations  13.5 us (15%)
  matrix products  7.91 us (9%)
  starting transfers between devices  5.82 us (7%)
  other arithmetic  2.42 us (3%)
  local copies, waits for them, and re-layouts  1.65 us (2%)
    all_to_all x1, blocking collectives, shards(): lax.all_to_all(outgoing.reshape(expert_count, capacity, hidden_state.shap...  21.7 us
    all_to_all x1, waiting for transfers between devices, shards(): lax.all_to_all(answers, 'ep', split_axis=0, concat_axis=0, tiled=True)  14.8 us
    reduce_scatter x1, waiting for transfers between devices, expert_rows(): lax.psum_scatter(partial_value.reshape(sources, item_count, feature_count...  9.7 us
    all_gather x1, waiting for transfers between devices, shards(): lax.all_gather(lax.all_to_all(outgoing.reshape(expert_count, capacity, hi...  8.17 us
    all_to_all x1, starting transfers between devices, shards(): lax.all_to_all(answers, 'ep', split_axis=0, concat_axis=0, tiled=True)  5.78 us
    dot_general x1, matrix products, expert_rows(): jnp.dot(token_rows, gate_matrix[0], preferred_element_type=jnp.float32)  2.62 us
    psum x1, blocking collectives, shards(): total_squares = lax.psum(local_squares, 'tp')  2.47 us
    dot_general x1, matrix products, expert_rows(): jnp.dot(activated, down_matrix[0], preferred_element_type=jnp.float32)  2.24 us
  transfers between devices with their start and end apart: 3, of which 3 were waited for; matrix products, arithmetic and copies ran while one was open for 0% of the time, Pallas kernels for 0%

commit v1 on v0

--- a/solution.py
+++ b/solution.py
@@ -5,6 +5,11 @@
 
 D = 1024
 norm_eps = 1e-05
+
+
+def gather_over(x, axis, dim):
+    sent = jnp.stack([x] * lax.axis_size(axis))
+    return jnp.concatenate(lax.all_to_all(sent, axis, 0, 0), axis=dim)
 
 
 def slot_numbers(block_ids, expert_count):
@@ -44,7 +49,7 @@
         jnp.bfloat16
     )
     answers = expert_rows(
-        lax.all_gather(
+        gather_over(
             lax.all_to_all(
                 outgoing.reshape(expert_count, capacity, hidden_state.shape[1]),
                 "ep",
@@ -53,8 +58,7 @@
                 tiled=True,
             ),
             "tp",
-            axis=2,
-            tiled=True,
+            2,
         ),
         gate_matrix,
         up_matrix,

time: 88.5 us -> 83.1 us (0.939)
  waiting for transfers between devices: 32.7 us -> 22.4 us
  blocking collectives: 24.2 us -> 28.6 us
  local copies, waits for them, and re-layouts: 1.65 us -> 3.23 us
  matrix products: 7.91 us -> 6.62 us
    all_gather x1 -> x0, waiting for transfers between devices: 8.17 us -> none  [shards(): lax.all_gather(lax.all_to_all(outgoing.reshape(expert_count, capacity, hi...]
    all_to_all x0 -> x1, blocking collectives: none -> 4.58 us  [gather_over(): return jnp.concatenate(lax.all_to_all(sent, axis, 0, 0), axis=dim)]
    reduce_scatter x1, waiting for transfers between devices: 9.7 us -> 7.57 us  [expert_rows(): lax.psum_scatter(partial_value.reshape(sources, item_count, feature_count...]
    dot_general x1, matrix products: 2.62 us -> 1.27 us  [expert_rows(): jnp.dot(token_rows, gate_matrix[0], preferred_element_type=jnp.float32)]
    reshape x0 -> x1, local copies, waits for them, and re-layouts: none -> 1.08 us  [gather_over(): return jnp.concatenate(lax.all_to_all(sent, axis, 0, 0), axis=dim)]
  transfers between devices with their start and end apart: 3 -> 2, of which waited for: 3 -> 2; matrix products, arithmetic and copies ran while one was open for 0% -> 0% of each run, Pallas kernels for 0% -> 0%
where the time goes in v1:
time: 83.1 us; the launch traced here: 82.7 us
  blocking collectives  28.6 us (34%)
  waiting for transfers between devices  22.4 us (27%)
  between operations  13.5 us (16%)
  matrix products  6.62 us (8%)
  starting transfers between devices  5.79 us (7%)
  local copies, waits for them, and re-layouts  3.23 us (4%)
  other arithmetic  2.5 us (3%)
    all_to_all x1, blocking collectives, shards(): lax.all_to_all(outgoing.reshape(expert_count, capacity, hidden_state.shap...  21.6 us
    all_to_all x1, waiting for transfers between devices, shards(): lax.all_to_all(answers, 'ep', split_axis=0, concat_axis=0, tiled=True)  14.8 us
    reduce_scatter x1, waiting for transfers between devices, expert_rows(): lax.psum_scatter(partial_value.reshape(sources, item_count, feature_count...  7.57 us
    all_to_all x1, starting transfers between devices, shards(): lax.all_to_all(answers, 'ep', split_axis=0, concat_axis=0, tiled=True)  5.78 us
    all_to_all x1, blocking collectives, gather_over(): return jnp.concatenate(lax.all_to_all(sent, axis, 0, 0), axis=dim)  4.58 us
    psum x1, blocking collectives, shards(): total_squares = lax.psum(local_squares, 'tp')  2.47 us
    dot_general x1, matrix products, expert_rows(): jnp.dot(activated, down_matrix[0], preferred_element_type=jnp.float32)  2.25 us
  transfers between devices with their start and end apart: 2, of which 2 were waited for; matrix products, arithmetic and copies ran while one was open for 0% of the time, Pallas kernels for 0%

profile of v1, /device:TPU:0, one launch (start us, length us, event | category | flops | bytes accessed | tf_op | source)
XLA Modules:
  0.0 82.7 jit_solution(12229881236951380764)
XLA Ops:
  6.5 0.9 %copy.24 = s32[64,4]{1,0:T(8,128)S(1)} copy(s32[64,4]{0,1:T(4,128)} %param.8) | data formatting | bytes 2048 | tf_op args[1]
  7.5 0.1 eq.40
  7.6 0.6 reduce-window.6
  8.2 0.2 slice_reduce_fusion
  8.5 0.1 reshape.139
  8.7 0.7 multiply_add_fusion
  9.4 0.1 fusion.11
  9.5 1.2 %convolution_convert_fusion = bf16[512,512]{1,0:T(8,128)(2,1)S(1)} fusion(pred[64,512]{1,0:T(8,128)(4,1)S(1)} %fusion.11, bf16[64,512]{1,0:T(8,128)(2,1)} %param.7), kind=kOutput, calls=%fused_computation.8 | convolution fusion | flops 33816576 | bytes 622592 | tf_op jit(solution)/shard_map/dot_general | solution.py:48
  10.7 21.6 %all_to_all.15 = bf16[8,64,512]{2,1,0:T(8,128)(2,1)S(1)} all-to-all(bf16[8,64,512]{2,1,0:T(8,128)(2,1)S(1)} %bitcast.48), channel_id=1, replica_groups=mesh['grp'=2,'ep'=8,'tp'=2] {'ep'}, dimensions={0} | all-to-all | bytes 1048576 | tf_op jit(solution)/shard_map/all_to_all | solution.py:53
  32.4 4.6 %all_to_all.16 = bf16[2,8,64,512]{3,2,1,0:T(8,128)(2,1)S(1)} all-to-all(bf16[2,8,64,512]{3,2,1,0:T(8,128)(2,1)S(1)} %pad_maximum_fusion), channel_id=1, replica_groups=mesh['grp'=2,'ep'=8,'tp'=2] {'tp'}, dimensions={0} | all-to-all | bytes 2097152 | tf_op jit(solution)/shard_map/all_to_all | solution.py:12
  37.0 1.1 %copy.26 = bf16[8,64,2,512]{3,2,1,0:T(2,128)(2,1)S(1)} copy(bf16[8,64,2,512]{3,1,0,2:T(8,128)(2,1)S(1)} %bitcast.44) | data formatting | bytes 2097152 | tf_op jit(solution)/shard_map/reshape | solution.py:12
  38.1 0.2 copy.27
  38.4 1.3 %fusion.4 = f32[512,1024]{1,0:T(8,128)S(1)} fusion(bf16[512,1024]{1,0:T(8,128)(2,1)S(1)} %bitcast.49, bf16[1,1024,1024]{2,1,0:T(8,128)(2,1)S(1)} %copy-done), kind=kOutput, calls=%fused_computation.4 | convolution fusion | flops 1073741824 | bytes 5242880 | tf_op jit(solution)/shard_map/dot_general | solution.py:24
  39.6 0.3 copy-done.3
  39.9 1.4 %multiply_convert_fusion = bf16[512,1024]{1,0:T(8,128)(2,1)S(1)} fusion(f32[512,1024]{1,0:T(8,128)S(1)} %fusion.4, bf16[512,1024]{1,0:T(8,128)(2,1)S(1)} %bitcast.50, bf16[1,1024,1024]{2,1,0:T(8,128)(2,1)S(1)} %copy-done.3), kind=kOutput, calls=%fused_computation.6 | convolution fusion | flops 1076887552 | bytes 6291456 | tf_op jit(solution)/shard_map/dot_general | solution.py:25
  41.4 0.2 copy-done.4
  41.5 2.3 %fusion.8 = bf16[8,64,1024]{2,1,0:T(8,128)(2,1)} fusion(bf16[8,64,1024]{2,1,0:T(8,128)(2,1)S(1)} %bitcast.52, bf16[1,1024,1024]{2,1,0:T(8,128)(2,1)S(1)} %copy-done.4), kind=kOutput, calls=%fused_computation.7 | convolution fusion | flops 1074266112 | bytes 4194304 | tf_op jit(solution)/shard_map/dot_general | solution.py:27
  43.8 7.6 %reduce-scatter.2.cloned.1.call-done = bf16[8,64,512]{2,1,0:T(8,128)(2,1)} async-done(((bf16[8,64,1024]{2,1,0:T(8,128)(2,1)}), bf16[8,64,512]{2,1,0:T(8,128)(2,1)}) %reduce-scatter.2.cloned.1.call-update) | async-done | bytes 524304 | tf_op jit(solution)/shard_map/reduce_scatter | solution.py:28
  51.4 5.8 %all-to-all-start.2 = ((bf16[8,64,512]{2,1,0:T(8,128)(2,1)}), bf16[8,64,512]{2,1,0:T(8,128)(2,1)S(1)}, u32[]{:S(2)}, u32[]{:S(2)}) async-start(bf16[8,64,512]{2,1,0:T(8,128)(2,1)} %reduce-scatter.2.cloned.1.call-done), calls=%async_computation.3 | async-start | bytes 1048576 | tf_op jit(solution)/shard_map/all_to_all | solution.py:67
  57.2 0.1 select_reduce_fusion
  57.3 14.8 %all-to-all-done.2 = bf16[8,64,512]{2,1,0:T(8,128)(2,1)S(1)} async-done(((bf16[8,64,512]{2,1,0:T(8,128)(2,1)}), bf16[8,64,512]{2,1,0:T(8,128)(2,1)S(1)}, u32[]{:S(2)}, u32[]{:S(2)}) %all-to-all-start.2) | async-done | bytes 524320 | tf_op jit(solution)/shard_map/all_to_all | solution.py:67
  72.1 0.5 multiply_reduce_fusion
  72.6 2.5 %psum.7 = f32[64]{0:T(128)S(1)} all-reduce(f32[64]{0:T(128)S(1)} %get-tuple-element.5), channel_id=1, replica_groups=mesh['grp'=2,'ep'=8,'tp'=2] {'tp'}, use_global_device_ids=true, to_apply=%region_7.8 | all-reduce | flops 64 | bytes 512 | tf_op jit(solution)/shard_map/psum | solution.py:74
  75.1 0.7 multiply_convert_fusion.1
  (17 shorter events, 0.3 us)
Async XLA Ops:
  6.5 31.8 %copy-start = (bf16[1,1024,1024]{2,1,0:T(8,128)(2,1)S(1)}, bf16[1,1024,1024]{2,1,0:T(8,128)(2,1)}, u32[]{:S(2)}) copy-start(bf16[1,1024,1024]{2,1,0:T(8,128)(2,1)} %param.10) | copy-start | bytes 6291460
  6.5 44.9 %reduce-scatter.2.cloned.1.call-start = ((), (), s32[]{:S(2)}) async-start(), calls=%async_computation.4 | async-start | bytes 1572864 | tf_op jit(solution)/shard_map/reduce_scatter | solution.py:28
  38.4 1.6 %copy-start.3 = (bf16[1,1024,1024]{2,1,0:T(8,128)(2,1)S(1)}, bf16[1,1024,1024]{2,1,0:T(8,128)(2,1)}, u32[]{:S(2)}) copy-start(bf16[1,1024,1024]{2,1,0:T(8,128)(2,1)} %param.11) | copy-start | bytes 6291460
  39.9 1.6 %copy-start.4 = (bf16[1,1024,1024]{2,1,0:T(8,128)(2,1)S(1)}, bf16[1,1024,1024]{2,1,0:T(8,128)(2,1)}, u32[]{:S(2)}) copy-start(bf16[1,1024,1024]{2,1,0:T(8,128)(2,1)} %param.12) | copy-start | bytes 6291460
  43.8 13.4 %copy-start.1 = (f32[64,4]{0,1:T(4,128)S(1)}, f32[64,4]{0,1:T(4,128)}, u32[]{:S(2)}) copy-start(f32[64,4]{0,1:T(4,128)} %param.9) | copy-start | bytes 3076
  43.8 31.3 %copy-start.2 = (f32[512]{0:T(512)S(1)}, f32[512]{0:T(512)}, u32[]{:S(2)}) copy-start(f32[512]{0:T(512)} %param.13) | copy-start | bytes 6148
  51.4 20.7 %all-to-all-start.2 = ((bf16[8,64,512]{2,1,0:T(8,128)(2,1)}), bf16[8,64,512]{2,1,0:T(8,128)(2,1)S(1)}, u32[]{:S(2)}, u32[]{:S(2)}) async-start(bf16[8,64,512]{2,1,0:T(8,128)(2,1)} %reduce-scatter.2.cloned.1.call-done), calls=%async_computation.3 | async-start | bytes 1048576 | tf_op jit(solution)/shard_map/all_to_all | solution.py:67
Sparse Core Ops, SparseCore 0:
  43.9 7.4 reduce-scatter.1
